TPU v7x, 256 devices: a 4x2x16 block of a 4x16x16 slice. The times are simulated.
256 devices in a mesh: grp: 2 (over y), sp: 32 (over z, core), tp: 4 (over x).
Axes of the slice: x: 4, y: 2, z: 16, core: 2. Of those that a mesh axis runs over, the one named last changes fastest.
The devices are a block of a 4x16x16 slice.
Arguments:
- query_nope: bfloat16 [20480, 1024], P(('grp', 'sp'), 'tp'), parts along dimension 0, may hold values from -12 to 12
- query_rope: bfloat16 [20480, 512], P(('grp', 'sp'), 'tp'), parts along dimension 0, may hold values from -48 to 48
- token_latent: bfloat16 [20480, 256], P(('grp', 'sp')), parts along dimension 0, may hold values from -6 to 6
- key_rope: bfloat16 [20480, 32], P(('grp', 'sp')), parts along dimension 0, may hold values from -48 to 48
- latent_norm_gain: float32 [256], replicated, may hold values from 0.1 to 1.9
- key_expand_weight: bfloat16 [256, 1024], replicated, may hold values from -0.375 to 0.375
- value_expand_weight: bfloat16 [256, 1024], replicated, may hold values from -0.375 to 0.375
- residual: bfloat16 [20480, 2048], P(('grp', 'sp')), parts along dimension 0, may hold values from -3 to 3
- out_weight: bfloat16 [1024, 2048], P('tp'), may hold values from -0.375 to 0.375
- ffn_gain: float32 [2048], replicated, may hold values from 0.1 to 1.9
- gate_weight: bfloat16 [2048, 5632], P('sp', 'tp'), may hold values from -0.125 to 0.125
- up_weight: bfloat16 [2048, 5632], P('sp', 'tp'), may hold values from -0.125 to 0.125
- down_weight: bfloat16 [5632, 2048], P('tp', 'sp'), may hold values from -0.078125 to 0.078125
Outputs:
- layer_output: bfloat16 [20480, 2048], P(('grp', 'sp', 'tp')), parts along dimension 0
There are 2 independent parts, one for each index of `grp`. A program takes and returns all parts, laid end to end along the dimension named above; an argument that names none is the same for every part. Nothing has to cross between parts.
All inputs are finite; a program needn't handle non-finite values.
Results may differ from a plain program's by a relative error of at most 0.015.
Values may be sent and summed in bfloat16 or wider, within the bound.
No kernel may reach another device: no remote copies, remote signals or barrier semaphores. Data moves between devices by JAX's collectives and lax.ppermute only.
A program may use at most 128 MiB of HBM per device.

v0:
```python
import jax
import jax.numpy as jnp
from jax import lax
from jax.sharding import PartitionSpec as P

UNROTATED_SIZE = 64
ROPE = 32
VALUE_SIZE = 64
GRID_W = 64


def side_by_side(arrays, axis, dim, along):
    widths = [a.shape[along] for a in arrays]
    both = jnp.concatenate(arrays, axis=along)
    whole = lax.all_gather(both, axis, axis=dim, tiled=True)
    return tuple(jnp.split(whole, [sum(widths[:k]) for k in range(1, len(widths))], axis=along))


def cut_along(array, dim, count):
    dims = array.shape
    parts = array.reshape(*dims[:dim], count, dims[dim] // count, *dims[dim + 1 :])
    return jnp.moveaxis(parts, dim, 0)


def summed_on_arrival(array, axis, dim):
    count = lax.axis_size(axis)
    parts = lax.all_to_all(cut_along(array, dim, count), axis, 0, 0, tiled=True)
    return jnp.sum(parts.astype(jnp.float32), axis=0)


def sent_to_all(array, axis):
    copies = jnp.broadcast_to(array, (lax.axis_size(axis), *array.shape))
    return lax.all_to_all(copies, axis, split_axis=0, concat_axis=0, tiled=True)


def joined_along(parts, dim):
    dims = list(parts.shape[1:])
    dims[dim] *= parts.shape[0]
    return jnp.moveaxis(parts, 0, dim).reshape(dims)


def collect(array, axis, dim):
    parts = sent_to_all(array, axis)
    return joined_along(parts, dim)


def norm_rows(values, gain):
    wide = values.astype(jnp.float32)
    return wide * lax.rsqrt(jnp.mean(wide * wide, axis=-1, keepdims=True) + 1e-06) * gain


def turn_heads(vectors, positions):
    tokens, heads, width = vectors.shape
    freqs = width // 4
    grid_pos = jnp.stack([positions // GRID_W, positions % GRID_W], axis=-1).astype(jnp.float32)
    inverse = jnp.power(10000.0, -jnp.arange(freqs, dtype=jnp.float32) / freqs)
    angles = grid_pos[:, :, None] * inverse
    cosine = jnp.cos(angles)[:, None]
    sine = jnp.sin(angles)[:, None]
    viewed = vectors.reshape(tokens, heads, 2, 2, freqs)
    first = viewed[..., 0, :]
    second = viewed[..., 1, :]
    turned = jnp.stack([first * cosine - second * sine, first * sine + second * cosine], axis=-2)
    return turned.reshape(tokens, heads, width)


def local(
    query_nope,
    query_rope,
    token_latent,
    key_rope,
    latent_norm_gain,
    key_expand_weight,
    value_expand_weight,
    residual,
    out_weight,
    ffn_gain,
    gate_weight,
    up_weight,
    down_weight,
):
    tok_rows = query_nope.shape[0]
    heads_here = query_nope.shape[1] // UNROTATED_SIZE
    own_rows = tok_rows // lax.axis_size("tp")
    tp_index = lax.axis_index("tp")
    positions = lax.axis_index("sp") * tok_rows + jnp.arange(tok_rows, dtype=jnp.int32)
    gate_full, up_full = side_by_side((gate_weight, up_weight), "sp", 0, 1)
    query_flat = query_nope.reshape(tok_rows, heads_here, UNROTATED_SIZE)
    query_turned = turn_heads(
        query_rope.astype(jnp.float32).reshape(tok_rows, heads_here, ROPE), positions
    ).astype(jnp.bfloat16)
    latent = norm_rows(token_latent, latent_norm_gain).astype(jnp.bfloat16)
    key_turned = turn_heads(key_rope.astype(jnp.float32)[:, None, :], positions)[:, 0].astype(
        jnp.bfloat16
    )
    key_cols = lax.dynamic_slice_in_dim(
        key_expand_weight, tp_index * heads_here * UNROTATED_SIZE, heads_here * UNROTATED_SIZE, 1
    )
    value_cols = lax.dynamic_slice_in_dim(
        value_expand_weight, tp_index * heads_here * VALUE_SIZE, heads_here * VALUE_SIZE, 1
    )
    score_scale = (UNROTATED_SIZE + ROPE) ** (-0.5)

    def absorb(carried, block_in):
        latent_block, rope_block = block_in
        block_rows = latent_block.shape[0]
        key_rows = jnp.dot(latent_block, key_cols, preferred_element_type=jnp.float32).astype(
            jnp.bfloat16
        )
        key_rows = key_rows.reshape(block_rows, heads_here, UNROTATED_SIZE)
        value_rows = jnp.dot(latent_block, value_cols, preferred_element_type=jnp.float32).astype(
            jnp.bfloat16
        )
        value_rows = value_rows.reshape(block_rows, heads_here, VALUE_SIZE)
        scores = (
            jnp.einsum("qhd,khd->hqk", query_flat, key_rows, preferred_element_type=jnp.float32)
            + jnp.einsum(
                "qhd,kd->hqk", query_turned, rope_block, preferred_element_type=jnp.float32
            )
        ) * score_scale
        highest, totals, accumulated = carried
        new_highest = jnp.maximum(highest, jnp.max(scores, axis=-1))
        shrink = jnp.exp(highest - new_highest)
        weights = jnp.exp(scores - new_highest[:, :, None])
        totals = totals * shrink + jnp.sum(weights, axis=-1)
        accumulated = accumulated * shrink.T[:, :, None] + jnp.einsum(
            "hqk,khd->qhd",
            weights.astype(jnp.bfloat16),
            value_rows,
            preferred_element_type=jnp.float32,
        )
        return ((new_highest, totals, accumulated), None)

    initial = (
        jnp.full((heads_here, tok_rows), -jnp.inf, jnp.float32),
        jnp.zeros((heads_here, tok_rows), jnp.float32),
        jnp.zeros((tok_rows, heads_here, VALUE_SIZE), jnp.float32),
    )
    carried = initial
    latent_piece = lax.all_gather(latent, "sp", axis=0, tiled=True)
    rope_piece = lax.all_gather(key_turned, "sp", axis=0, tiled=True)
    shard_count = latent_piece.shape[0] // tok_rows
    grouped = max(
        (
            factor
            for factor in range(1, shard_count + 1)
            if shard_count % factor == 0 and factor * tok_rows <= max(1024, tok_rows)
        )
    )
    block_rows = grouped * tok_rows
    blocks = (
        latent_piece.reshape(-1, block_rows, latent_piece.shape[1]),
        rope_piece.reshape(-1, block_rows, rope_piece.shape[1]),
    )
    carried, _ = lax.scan(absorb, carried, blocks)
    highest, totals, accumulated = carried
    attended = (
        (accumulated / totals.T[:, :, None])
        .reshape(tok_rows, heads_here * VALUE_SIZE)
        .astype(jnp.bfloat16)
    )
    head_sum = summed_on_arrival(
        jnp.dot(attended, out_weight, preferred_element_type=jnp.float32).astype(jnp.bfloat16),
        "tp",
        0,
    )
    mixed_own = (
        lax.dynamic_slice_in_dim(residual, tp_index * own_rows, own_rows, 0).astype(jnp.float32)
        + head_sum
    )
    normed_own = norm_rows(mixed_own, ffn_gain).astype(jnp.bfloat16)
    normed_all = collect(normed_own, "tp", 0)
    gate = jnp.dot(normed_all, gate_full, preferred_element_type=jnp.float32)
    up_part = jnp.dot(normed_all, up_full, preferred_element_type=jnp.float32)
    hidden = (jax.nn.silu(gate) * up_part).astype(jnp.bfloat16)
    terms = jnp.dot(
        hidden,
        lax.all_gather(down_weight, "sp", axis=1, tiled=True),
        preferred_element_type=jnp.float32,
    )
    ffn_own = summed_on_arrival(terms.astype(jnp.bfloat16), "tp", 0)
    return (mixed_own + ffn_own).astype(jnp.bfloat16)


def solution(mesh):
    return jax.shard_map(
        local,
        mesh=mesh,
        in_specs=(
            P(("grp", "sp"), "tp"),
            P(("grp", "sp"), "tp"),
            P(("grp", "sp"), None),
            P(("grp", "sp"), None),
            P(),
            P(),
            P(),
            P(("grp", "sp"), None),
            P("tp", None),
            P(),
            P("sp", "tp"),
            P("sp", "tp"),
            P("tp", "sp"),
        ),
        out_specs=P(("grp", "sp", "tp"), None),
        check_vma=False,
    )
```

profile of v0, /device:TPU:40, one launch (start us, length us, event | category | flops | bytes accessed | tf_op | source)
XLA Modules:
  0.0 341.1 jit_solution(13385910839321723179)
XLA Ops:
  7.7 1.7 fusion.38
  9.6 1.8 pad_maximum_fusion
  15.8 52.6 %all-gather = bf16[32,320,32]{1,2,0:T(8,128)(2,1)S(1)} all-gather(bf16[1,320,32]{1,2,0:T(8,128)(2,1)S(1)} %bitcast.89), channel_id=1, replica_groups=mesh['grp'=2,'sp'=32,'tp'=4] {'sp'}, dimensions={0}, use_global_device_ids=true | all-gather | bytes 675840 | tf_op jit(solution)/shard_map/all_gather | solution.py:141
  72.4 24.7 %all-gather.5.cloned.1.call-done = bf16[10240,256]{1,0:T(8,128)(2,1)} async-done(((bf16[320,256]{1,0:T(8,128)(2,1)}), bf16[10240,256]{1,0:T(8,128)(2,1)}) %all-gather.5.cloned.1.call-update) | async-done | bytes 5242896 | tf_op jit(solution)/shard_map/all_gather | solution.py:140
  97.1 152.5 %while.15 = (s32[]{:T(128)}, f32[4,320]{1,0:T(4,128)S(1)}, f32[4,320]{1,0:T(4,128)S(1)}, f32[320,4,64]{0,2,1:T(8,128)S(1)}, bf16[16,640,256]{2,1,0:T(8,128)(2,1)...) while((s32[]{:T(128)}, f32[4,320]{1,0:T(4,128)S(1)}, ...), condition=%wide.region_4.5_spmd.clone, body=%wide.region_1.4_spmd.clone.sunk | while | flops 436231680 | bytes 32760992 | solution.py:155
  99.0 2.4 fusion.86
  101.4 1.4 convolution_convert_fusion.7
  102.9 2.7 fusion.90
  108.5 2.4 fusion.86
  110.9 1.4 convolution_convert_fusion.7
  112.4 2.7 fusion.90
  118.0 2.4 fusion.86
  120.4 1.4 convolution_convert_fusion.7
  121.9 2.8 fusion.90
  127.5 2.4 fusion.86
  130.0 1.4 convolution_convert_fusion.7
  131.4 2.7 fusion.90
  135.1 1.3 convolution_convert_fusion.6
  137.0 2.4 fusion.86
  139.5 1.4 convolution_convert_fusion.7
  140.9 2.8 fusion.90
  144.7 1.3 convolution_convert_fusion.6
  146.6 2.4 fusion.86
  149.0 1.4 convolution_convert_fusion.7
  150.5 2.8 fusion.90
  154.2 1.3 convolution_convert_fusion.6
  156.2 2.4 fusion.86
  158.6 1.4 convolution_convert_fusion.7
  160.1 2.8 fusion.90
  165.7 2.4 fusion.86
  168.2 1.4 convolution_convert_fusion.7
  169.6 2.8 fusion.90
  175.3 2.4 fusion.86
  177.7 1.4 convolution_convert_fusion.7
  179.2 2.7 fusion.90
  184.8 2.4 fusion.86
  187.2 1.4 convolution_convert_fusion.7
  188.7 2.9 fusion.90
  194.4 2.4 fusion.86
  196.8 1.4 convolution_convert_fusion.7
  198.3 2.8 fusion.90
  203.9 2.4 fusion.86
  206.4 1.4 convolution_convert_fusion.7
  207.8 2.7 fusion.90
  213.4 2.4 fusion.86
  215.9 1.4 convolution_convert_fusion.7
  217.3 2.8 fusion.90
  223.0 2.4 fusion.86
  225.4 1.4 convolution_convert_fusion.7
  226.8 2.8 fusion.90
  232.5 2.4 fusion.86
  235.0 1.4 convolution_convert_fusion.7
  236.4 2.7 fusion.90
  242.0 2.4 fusion.86
  244.4 1.4 convolution_convert_fusion.7
  245.9 2.8 fusion.90
  249.6 1.6 convolution_convert_fusion.3
  251.2 4.2 %all-to-all-start = ((bf16[4,80,2048]{2,1,0:T(8,128)(2,1)}), bf16[4,80,2048]{2,1,0:T(8,128)(2,1)S(1)}, u32[]{:S(2)}, u32[]{:S(2)}) async-start(bf16[4,80,2048]{2,1,0:T(8,128)(2,1)} %bitcast.80), calls=%async_computation | async-start | bytes 2621440 | tf_op jit(solution)/shard_map/all_to_all | solution.py:27
  255.4 18.3 %all-to-all-done = bf16[4,80,2048]{2,1,0:T(8,128)(2,1)S(1)} async-done(((bf16[4,80,2048]{2,1,0:T(8,128)(2,1)}), bf16[4,80,2048]{2,1,0:T(8,128)(2,1)S(1)}, u32[]{:S(2)}, u32[]{:S(2)}) %all-to-all-start) | async-done | bytes 1310752 | tf_op jit(solution)/shard_map/all_to_all | solution.py:27
  276.4 20.0 %all_to_all.15 = bf16[4,80,2048]{2,1,0:T(8,128)(2,1)S(1)} all-to-all(bf16[4,80,2048]{2,1,0:T(8,128)(2,1)S(1)} %broadcast_in_dim.11), channel_id=1, replica_groups=mesh['grp'=2,'sp'=32,'tp'=4] {'tp'}, dimensions={0} | all-to-all | bytes 2621440 | tf_op jit(solution)/shard_map/all_to_all | solution.py:33
  296.4 6.1 %fusion.25 = f32[320,1408]{1,0:T(8,128)} fusion(bf16[320,2048]{1,0:T(8,128)(2,1)S(1)} %bitcast.83, bf16[2048,2816]{1,0:T(8,128)(2,1)} %all-gather.7.cloned.1.call-done), kind=kOutput, calls=%fused_computation.28 | convolution fusion | flops 1845493760 | bytes 8880128 | tf_op jit(solution)/shard_map/dot_general | solution.py:173
  302.5 10.2 %convolution_convert_fusion.2 = bf16[320,2048]{1,0:T(8,128)(2,1)} fusion(bf16[1408,2048]{0,1:T(8,128)(2,1)} %all-gather.9.cloned.1.call-done, bf16[320,2048]{1,0:T(8,128)(2,1)S(1)} %bitcast.84, bf16[2048,2816]{1,0:T(8,128)(2,1)} %all-gather.7.cloned.1.call-done, f32[320,1408]{1,0:T(8,128)} %fusion.25), kind=kOutput, calls=%fused_computation.31 | convolution fusion | flops 3694346240 | bytes 15958016 | tf_op jit(solution)/shard_map/dot_general | solution.py:176
  312.6 19.9 %all_to_all.16 = bf16[4,80,2048]{2,1,0:T(8,128)(2,1)S(1)} all-to-all(bf16[4,80,2048]{2,1,0:T(8,128)(2,1)} %bitcast.85), channel_id=1, replica_groups=mesh['grp'=2,'sp'=32,'tp'=4] {'tp'}, dimensions={0} | all-to-all | bytes 2621440 | tf_op jit(solution)/shard_map/all_to_all | solution.py:27
  332.7 1.8 add_convert_fusion
  (165 shorter events, 53.8 us)
Async XLA Ops:
  6.5 243.1 %copy-start = (bf16[256,2048]{1,0:T(8,128)(2,1)S(1)}, bf16[256,2048]{1,0:T(8,128)(2,1)}, u32[]{:S(2)}) copy-start(bf16[256,2048]{1,0:T(8,128)(2,1)} %param.23) | copy-start | bytes 3145732
  6.6 90.5 %all-gather.5.cloned.1.call-start = ((), (), s32[]{:S(2)}) async-start(), calls=%async_computation.3 | async-start | bytes 5406720 | tf_op jit(solution)/shard_map/all_gather | solution.py:140
  9.5 286.9 %all-gather.7.cloned.1.call-start = ((), (), s32[]{:S(2)}) async-start(), calls=%async_computation.4 | async-start | bytes 11894784 | tf_op jit(solution)/shard_map/all_gather | solution.py:15
  11.4 291.0 %all-gather.9.cloned.1.call-start = ((), (), s32[]{:S(2)}) async-start(), calls=%async_computation.5 | async-start | bytes 5947392 | tf_op jit(solution)/shard_map/all_gather | solution.py:178
  101.4 4.2 %copy-start.1 = (f32[4,320,640]{2,1,0:T(8,128)S(1)}, f32[4,320,640]{2,1,0:T(8,128)}, u32[]{:S(2)}) copy-start(f32[4,320,640]{2,1,0:T(8,128)} %get-tuple-element.224) | copy-start | bytes 9830404 | tf_op jit(solution)/shard_map/while
  110.9 4.2 %copy-start.1 = (f32[4,320,640]{2,1,0:T(8,128)S(1)}, f32[4,320,640]{2,1,0:T(8,128)}, u32[]{:S(2)}) copy-start(f32[4,320,640]{2,1,0:T(8,128)} %get-tuple-element.224) | copy-start | bytes 9830404 | tf_op jit(solution)/shard_map/while
  120.4 4.3 %copy-start.1 = (f32[4,320,640]{2,1,0:T(8,128)S(1)}, f32[4,320,640]{2,1,0:T(8,128)}, u32[]{:S(2)}) copy-start(f32[4,320,640]{2,1,0:T(8,128)} %get-tuple-element.224) | copy-start | bytes 9830404 | tf_op jit(solution)/shard_map/while
  130.0 4.2 %copy-start.1 = (f32[4,320,640]{2,1,0:T(8,128)S(1)}, f32[4,320,640]{2,1,0:T(8,128)}, u32[]{:S(2)}) copy-start(f32[4,320,640]{2,1,0:T(8,128)} %get-tuple-element.224) | copy-start | bytes 9830404 | tf_op jit(solution)/shard_map/while
  139.5 4.3 %copy-start.1 = (f32[4,320,640]{2,1,0:T(8,128)S(1)}, f32[4,320,640]{2,1,0:T(8,128)}, u32[]{:S(2)}) copy-start(f32[4,320,640]{2,1,0:T(8,128)} %get-tuple-element.224) | copy-start | bytes 9830404 | tf_op jit(solution)/shard_map/while
  149.0 4.3 %copy-start.1 = (f32[4,320,640]{2,1,0:T(8,128)S(1)}, f32[4,320,640]{2,1,0:T(8,128)}, u32[]{:S(2)}) copy-start(f32[4,320,640]{2,1,0:T(8,128)} %get-tuple-element.224) | copy-start | bytes 9830404 | tf_op jit(solution)/shard_map/while
  158.6 4.3 %copy-start.1 = (f32[4,320,640]{2,1,0:T(8,128)S(1)}, f32[4,320,640]{2,1,0:T(8,128)}, u32[]{:S(2)}) copy-start(f32[4,320,640]{2,1,0:T(8,128)} %get-tuple-element.224) | copy-start | bytes 9830404 | tf_op jit(solution)/shard_map/while
  168.2 4.3 %copy-start.1 = (f32[4,320,640]{2,1,0:T(8,128)S(1)}, f32[4,320,640]{2,1,0:T(8,128)}, u32[]{:S(2)}) copy-start(f32[4,320,640]{2,1,0:T(8,128)} %get-tuple-element.224) | copy-start | bytes 9830404 | tf_op jit(solution)/shard_map/while
  177.7 4.2 %copy-start.1 = (f32[4,320,640]{2,1,0:T(8,128)S(1)}, f32[4,320,640]{2,1,0:T(8,128)}, u32[]{:S(2)}) copy-start(f32[4,320,640]{2,1,0:T(8,128)} %get-tuple-element.224) | copy-start | bytes 9830404 | tf_op jit(solution)/shard_map/while
  187.2 4.3 %copy-start.1 = (f32[4,320,640]{2,1,0:T(8,128)S(1)}, f32[4,320,640]{2,1,0:T(8,128)}, u32[]{:S(2)}) copy-start(f32[4,320,640]{2,1,0:T(8,128)} %get-tuple-element.224) | copy-start | bytes 9830404 | tf_op jit(solution)/shard_map/while
  196.8 4.2 %copy-start.1 = (f32[4,320,640]{2,1,0:T(8,128)S(1)}, f32[4,320,640]{2,1,0:T(8,128)}, u32[]{:S(2)}) copy-start(f32[4,320,640]{2,1,0:T(8,128)} %get-tuple-element.224) | copy-start | bytes 9830404 | tf_op jit(solution)/shard_map/while
  206.4 4.2 %copy-start.1 = (f32[4,320,640]{2,1,0:T(8,128)S(1)}, f32[4,320,640]{2,1,0:T(8,128)}, u32[]{:S(2)}) copy-start(f32[4,320,640]{2,1,0:T(8,128)} %get-tuple-element.224) | copy-start | bytes 9830404 | tf_op jit(solution)/shard_map/while
  215.9 4.2 %copy-start.1 = (f32[4,320,640]{2,1,0:T(8,128)S(1)}, f32[4,320,640]{2,1,0:T(8,128)}, u32[]{:S(2)}) copy-start(f32[4,320,640]{2,1,0:T(8,128)} %get-tuple-element.224) | copy-start | bytes 9830404 | tf_op jit(solution)/shard_map/while
  225.4 4.2 %copy-start.1 = (f32[4,320,640]{2,1,0:T(8,128)S(1)}, f32[4,320,640]{2,1,0:T(8,128)}, u32[]{:S(2)}) copy-start(f32[4,320,640]{2,1,0:T(8,128)} %get-tuple-element.224) | copy-start | bytes 9830404 | tf_op jit(solution)/shard_map/while
  234.9 4.2 %copy-start.1 = (f32[4,320,640]{2,1,0:T(8,128)S(1)}, f32[4,320,640]{2,1,0:T(8,128)}, u32[]{:S(2)}) copy-start(f32[4,320,640]{2,1,0:T(8,128)} %get-tuple-element.224) | copy-start | bytes 9830404 | tf_op jit(solution)/shard_map/while
  244.4 4.2 %copy-start.1 = (f32[4,320,640]{2,1,0:T(8,128)S(1)}, f32[4,320,640]{2,1,0:T(8,128)}, u32[]{:S(2)}) copy-start(f32[4,320,640]{2,1,0:T(8,128)} %get-tuple-element.224) | copy-start | bytes 9830404 | tf_op jit(solution)/shard_map/while
  251.2 23.9 %copy-start.2 = (f32[2048]{0:T(1024)S(1)}, f32[2048]{0:T(1024)}, u32[]{:S(2)}) copy-start(f32[2048]{0:T(1024)} %param.24) | copy-start | bytes 24580
  251.2 22.5 %all-to-all-start = ((bf16[4,80,2048]{2,1,0:T(8,128)(2,1)}), bf16[4,80,2048]{2,1,0:T(8,128)(2,1)S(1)}, u32[]{:S(2)}, u32[]{:S(2)}) async-start(bf16[4,80,2048]{2,1,0:T(8,128)(2,1)} %bitcast.80), calls=%async_computation | async-start | bytes 2621440 | tf_op jit(solution)/shard_map/all_to_all | solution.py:27
Sparse Core Ops, SparseCore 0:
  9.6 87.3 all-gather.4
  98.9 77.7 all-gather.6
  178.5 70.0 all-gather.8
where the time goes:
time: 343 us; the launch traced here: 341 us
  matrix products  155 us (45%)
  blocking collectives  92.5 us (27%)
  waiting for transfers between devices  43.8 us (13%)
  other arithmetic  27.3 us (8%)
  between operations  13.3 us (4%)
  starting transfers between devices  4.32 us (1%)
  local copies, waits for them, and re-layouts  4.2 us (1%)
    all_gather x1, blocking collectives, local(): rope_piece = lax.all_gather(key_turned, 'sp', axis=0, tiled=True)  52.6 us
    dot_general x16, matrix products, absorb(): jnp.einsum('hqk,khd->qhd', weights.astype(jnp.bfloat16), value_rows, pref...  44.4 us
    dot_general x16, matrix products, absorb(): jnp.einsum('qhd,kd->hqk', query_turned, rope_block, preferred_element_typ...  39 us
    all_gather x1, waiting for transfers between devices, local(): latent_piece = lax.all_gather(latent, 'sp', axis=0, tiled=True)  24.7 us
    dot_general x16, matrix products, absorb(): jnp.dot(latent_block, value_cols, preferred_element_type=jnp.float32)  22.9 us
    dot_general x16, matrix products, absorb(): jnp.dot(latent_block, key_cols, preferred_element_type=jnp.float32)  20.4 us
    all_to_all x1, blocking collectives, sent_to_all(): return lax.all_to_all(copies, axis, split_axis=0, concat_axis=0, tiled=True)  20 us
    all_to_all x1, blocking collectives, summed_on_arrival(): parts = lax.all_to_all(cut_along(array, dim, count), axis, 0, 0, tiled=True)  19.9 us
  transfers between devices with their start and end apart: 4, of which 2 were waited for; matrix products, arithmetic and copies ran while one was open for 50% of the time, Pallas kernels for 0%

commit v1 on v0

--- a/solution.py
+++ b/solution.py
@@ -7,6 +7,13 @@
 ROPE = 32
 VALUE_SIZE = 64
 GRID_W = 64
+
+
+def exchange_gather(x, name, dim):
+    peers = lax.axis_size(name)
+    blocks = jnp.stack([x for _ in range(peers)])
+    blocks = lax.all_to_all(blocks, name, split_axis=0, concat_axis=0)
+    return jnp.concatenate(blocks, axis=dim)
 
 
 def side_by_side(arrays, axis, dim, along):
@@ -137,7 +144,7 @@
         jnp.zeros((tok_rows, heads_here, VALUE_SIZE), jnp.float32),
     )
     carried = initial
-    latent_piece = lax.all_gather(latent, "sp", axis=0, tiled=True)
+    latent_piece = exchange_gather(latent, "sp", 0)
     rope_piece = lax.all_gather(key_turned, "sp", axis=0, tiled=True)
     shard_count = latent_piece.shape[0] // tok_rows
     grouped = max(

time: 343 us -> 600 us (1.75)
  blocking collectives: 92.5 us -> 348 us
  starting transfers between devices: 4.32 us -> 29.5 us
  waiting for transfers between devices: 43.8 us -> 19.1 us
    all_gather x1, blocking collectives: 52.6 us -> 308 us  [local(): rope_piece = lax.all_gather(key_turned, 'sp', axis=0, tiled=True)]
    all_to_all x0 -> x1, starting transfers between devices: none -> 24.9 us  [exchange_gather(): blocks = lax.all_to_all(blocks, name, split_axis=0, concat_axis=0)]
    all_gather x1 -> x0, waiting for transfers between devices: 24.7 us -> none  [local(): latent_piece = lax.all_gather(latent, 'sp', axis=0, tiled=True)]
  transfers between devices with their start and end apart: 4 -> 4, of which waited for: 2 -> 1; matrix products, arithmetic and copies ran while one was open for 50% -> 29% of each run, Pallas kernels for 0% -> 0%
where the time goes in v1:
time: 600 us; the launch traced here: 598 us
  blocking collectives  348 us (58%)
  matrix products  154 us (26%)
  starting transfers between devices  29.5 us (5%)
  other arithmetic  25.9 us (4%)
  waiting for transfers between devices  19.1 us (3%)
  between operations  13.7 us (2%)
  local copies, waits for them, and re-layouts  6.67 us (1%)
    all_gather x1, blocking collectives, local(): rope_piece = lax.all_gather(key_turned, 'sp', axis=0, tiled=True)  308 us
    dot_general x16, matrix products, absorb(): jnp.einsum('hqk,khd->qhd', weights.astype(jnp.bfloat16), value_rows, pref...  43.9 us
    dot_general x16, matrix products, absorb(): jnp.einsum('qhd,kd->hqk', query_turned, rope_block, preferred_element_typ...  39.1 us
    all_to_all x1, starting transfers between devices, exchange_gather(): blocks = lax.all_to_all(blocks, name, split_axis=0, concat_axis=0)  24.9 us
    dot_general x16, matrix products, absorb(): jnp.dot(latent_block, value_cols, preferred_element_type=jnp.float32)  22.8 us
    dot_general x16, matrix products, absorb(): jnp.dot(latent_block, key_cols, preferred_element_type=jnp.float32)  20.4 us
    all_to_all x1, blocking collectives, sent_to_all(): return lax.all_to_all(copies, axis, split_axis=0, concat_axis=0, tiled=True)  19.9 us
    all_to_all x1, blocking collectives, summed_on_arrival(): parts = lax.all_to_all(cut_along(array, dim, count), axis, 0, 0, tiled=True)  19.9 us
  transfers between devices with their start and end apart: 4, of which 1 were waited for; matrix products, arithmetic and copies ran while one was open for 29% of the time, Pallas kernels for 0%

profile of v1, /device:TPU:40, one launch (start us, length us, event | category | flops | bytes accessed | tf_op | source)
XLA Modules:
  0.0 597.8 jit_solution(10977336075720100528)
XLA Ops:
  6.6 1.9 pad_maximum_fusion
  10.6 3.0 stack.10
  13.6 24.9 %all-to-all-start = ((bf16[32,320,256]{2,1,0:T(8,128)(2,1)}), bf16[32,320,256]{2,1,0:T(8,128)(2,1)}, u32[]{:S(2)}, u32[]{:S(2)}) async-start(bf16[32,320,256]{2,1,0:T(8,128)(2,1)} %stack.10), calls=%async_computation | async-start | bytes 10485760 | tf_op jit(solution)/shard_map/all_to_all | solution.py:15
  40.8 308.0 %all-gather = bf16[32,320,32]{1,2,0:T(8,128)(2,1)S(1)} all-gather(bf16[1,320,32]{1,2,0:T(8,128)(2,1)S(1)} %bitcast.88), channel_id=1, replica_groups=mesh['grp'=2,'sp'=32,'tp'=4] {'sp'}, dimensions={0}, use_global_device_ids=true | all-gather | bytes 675840 | tf_op jit(solution)/shard_map/all_gather | solution.py:148
  353.7 152.0 %while.15 = (s32[]{:T(128)}, f32[4,320]{1,0:T(4,128)S(1)}, f32[4,320]{1,0:T(4,128)S(1)}, f32[320,4,64]{0,2,1:T(8,128)S(1)}, bf16[16,640,256]{2,1,0:T(8,128)(2,1)...) while((s32[]{:T(128)}, f32[4,320]{1,0:T(4,128)S(1)}, ...), condition=%wide.region_4.5_spmd.clone, body=%wide.region_1.4_spmd.clone.sunk | while | flops 436231680 | bytes 32760992 | solution.py:162
  355.6 2.4 fusion.86
  358.1 1.4 convolution_convert_fusion.7
  359.5 2.7 fusion.90
  363.2 1.3 convolution_convert_fusion.6
  365.1 2.4 fusion.86
  367.6 1.4 convolution_convert_fusion.7
  369.0 2.8 fusion.90
  372.8 1.3 convolution_convert_fusion.6
  374.7 2.4 fusion.86
  377.1 1.4 convolution_convert_fusion.7
  378.6 2.7 fusion.90
  384.2 2.4 fusion.86
  386.7 1.4 convolution_convert_fusion.7
  388.1 2.8 fusion.90
  391.8 1.3 convolution_convert_fusion.6
  393.7 2.4 fusion.86
  396.2 1.4 convolution_convert_fusion.7
  397.6 2.8 fusion.90
  403.2 2.4 fusion.86
  405.7 1.4 convolution_convert_fusion.7
  407.1 2.7 fusion.90
  412.7 2.4 fusion.86
  415.2 1.4 convolution_convert_fusion.7
  416.6 2.7 fusion.90
  422.2 2.4 fusion.86
  424.7 1.4 convolution_convert_fusion.7
  426.1 2.7 fusion.90
  431.7 2.4 fusion.86
  434.2 1.4 convolution_convert_fusion.7
  435.6 2.7 fusion.90
  441.2 2.4 fusion.86
  443.7 1.4 convolution_convert_fusion.7
  445.1 2.7 fusion.90
  450.7 2.4 fusion.86
  453.2 1.4 convolution_convert_fusion.7
  454.6 2.7 fusion.90
  460.2 2.4 fusion.86
  462.7 1.4 convolution_convert_fusion.7
  464.1 2.7 fusion.90
  469.7 2.4 fusion.86
  472.2 1.4 convolution_convert_fusion.7
  473.6 2.7 fusion.90
  479.2 2.4 fusion.86
  481.6 1.4 convolution_convert_fusion.7
  483.1 2.7 fusion.90
  488.7 2.4 fusion.86
  491.1 1.4 convolution_convert_fusion.7
  492.6 2.7 fusion.90
  498.2 2.4 fusion.86
  500.6 1.4 convolution_convert_fusion.7
  502.1 2.7 fusion.90
  505.8 1.6 convolution_convert_fusion.3
  507.4 4.5 all-to-all-start.1
  511.9 18.3 %all-to-all-done.1 = bf16[4,80,2048]{2,1,0:T(8,128)(2,1)S(1)} async-done(((bf16[4,80,2048]{2,1,0:T(8,128)(2,1)}), bf16[4,80,2048]{2,1,0:T(8,128)(2,1)S(1)}, u32[]{:S(2)}, u32[]{:S(2)}) %all-to-all-start.1) | async-done | bytes 1310752 | tf_op jit(solution)/shard_map/all_to_all | solution.py:34
  532.9 19.9 %all_to_all.20 = bf16[4,80,2048]{2,1,0:T(8,128)(2,1)S(1)} all-to-all(bf16[4,80,2048]{2,1,0:T(8,128)(2,1)S(1)} %broadcast_in_dim.11), channel_id=1, replica_groups=mesh['grp'=2,'sp'=32,'tp'=4] {'tp'}, dimensions={0} | all-to-all | bytes 2621440 | tf_op jit(solution)/shard_map/all_to_all | solution.py:40
  552.8 6.1 %fusion.25 = f32[320,1408]{1,0:T(8,128)} fusion(bf16[320,2048]{1,0:T(8,128)(2,1)S(1)} %bitcast.82, bf16[2048,2816]{1,0:T(8,128)(2,1)} %all-gather.4.cloned.1.call-done), kind=kOutput, calls=%fused_computation.28 | convolution fusion | flops 1845493760 | bytes 8880128 | tf_op jit(solution)/shard_map/dot_general | solution.py:180
  558.9 10.2 %convolution_convert_fusion.2 = bf16[320,2048]{1,0:T(8,128)(2,1)} fusion(bf16[1408,2048]{0,1:T(8,128)(2,1)} %all-gather.6.cloned.1.call-done, bf16[320,2048]{1,0:T(8,128)(2,1)S(1)} %bitcast.83, bf16[2048,2816]{1,0:T(8,128)(2,1)} %all-gather.4.cloned.1.call-done, f32[320,1408]{1,0:T(8,128)} %fusion.25), kind=kOutput, calls=%fused_computation.31 | convolution fusion | flops 3694346240 | bytes 15958016 | tf_op jit(solution)/shard_map/dot_general | solution.py:183
  569.1 19.9 %all_to_all.21 = bf16[4,80,2048]{2,1,0:T(8,128)(2,1)S(1)} all-to-all(bf16[4,80,2048]{2,1,0:T(8,128)(2,1)} %bitcast.84), channel_id=1, replica_groups=mesh['grp'=2,'sp'=32,'tp'=4] {'tp'}, dimensions={0} | all-to-all | bytes 2621440 | tf_op jit(solution)/shard_map/all_to_all | solution.py:34
  589.1 1.8 add_convert_fusion
  (173 shorter events, 53.5 us)
Async XLA Ops:
  6.5 499.2 %copy-start = (bf16[256,2048]{1,0:T(8,128)(2,1)S(1)}, bf16[256,2048]{1,0:T(8,128)(2,1)}, u32[]{:S(2)}) copy-start(bf16[256,2048]{1,0:T(8,128)(2,1)} %param.23) | copy-start | bytes 3145732
  6.6 546.3 %all-gather.4.cloned.1.call-start = ((), (), s32[]{:S(2)}) async-start(), calls=%async_computation.4 | async-start | bytes 11894784 | tf_op jit(solution)/shard_map/all_gather | solution.py:22
  13.6 25.8 %copy-start.2 = (bf16[320,128]{1,0:T(8,128)(2,1)S(1)}, bf16[320,128]{1,0:T(8,128)(2,1)}, u32[]{:S(2)}) copy-start(bf16[320,128]{1,0:T(8,128)(2,1)} %param.16) | copy-start | bytes 245764
  13.6 26.6 %copy-start.4 = (bf16[320,32]{0,1:T(8,128)(2,1)S(1)}, bf16[320,32]{0,1:T(8,128)(2,1)}, u32[]{:S(2)}) copy-start(bf16[320,32]{0,1:T(8,128)(2,1)} %param.18) | copy-start | bytes 61444
  13.6 340.1 %all-to-all-start = ((bf16[32,320,256]{2,1,0:T(8,128)(2,1)}), bf16[32,320,256]{2,1,0:T(8,128)(2,1)}, u32[]{:S(2)}, u32[]{:S(2)}) async-start(bf16[32,320,256]{2,1,0:T(8,128)(2,1)} %stack.10), calls=%async_computation | async-start | bytes 10485760 | tf_op jit(solution)/shard_map/all_to_all | solution.py:15
  38.5 520.4 %all-gather.6.cloned.1.call-start = ((), (), s32[]{:S(2)}) async-start(), calls=%async_computation.5 | async-start | bytes 5947392 | tf_op jit(solution)/shard_map/all_gather | solution.py:185
  40.2 0.6 copy-start.6
  40.3 0.6 copy-start.3
  358.1 4.2 copy-start.1
  367.6 4.2 copy-start.1
  377.1 4.2 copy-start.1
  386.6 4.2 copy-start.1
  396.2 4.2 copy-start.1
  405.7 4.2 copy-start.1
  415.2 4.2 copy-start.1
  424.7 4.2 copy-start.1
  434.2 4.2 copy-start.1
  443.7 4.2 copy-start.1
  453.1 4.2 copy-start.1
  462.6 4.2 copy-start.1
  472.1 4.2 copy-start.1
  481.6 4.2 copy-start.1
  491.1 4.2 copy-start.1
  500.6 4.2 copy-start.1
  507.4 24.2 %copy-start.5 = (f32[2048]{0:T(1024)S(1)}, f32[2048]{0:T(1024)}, u32[]{:S(2)}) copy-start(f32[2048]{0:T(1024)} %param.24) | copy-start | bytes 24580
  507.4 22.8 %all-to-all-start.1 = ((bf16[4,80,2048]{2,1,0:T(8,128)(2,1)}), bf16[4,80,2048]{2,1,0:T(8,128)(2,1)S(1)}, u32[]{:S(2)}, u32[]{:S(2)}) async-start(bf16[4,80,2048]{2,1,0:T(8,128)(2,1)} %bitcast.80), calls=%async_computation.1 | async-start | bytes 2621440 | tf_op jit(solution)/shard_map/all_to_all | solution.py:34
Sparse Core Ops, SparseCore 0:
  9.2 315.3 all-gather.3
  326.4 73.2 all-gather.5
